TPU v7x, 32 devices: a whole 2x2x4 slice. The times are simulated.
32 devices in a mesh: kv: 4 (over z), tp: 8 (over y, x, core).
Axes of the slice: x: 2, y: 2, z: 4, core: 2. Of those that a mesh axis runs over, the one named last changes fastest.
Arguments:
- piece_tokens: bfloat16 [512, 2048], P('kv'), may hold values from -6 to 6
- dec_tokens: bfloat16 [8, 2048], P('kv'), may hold values from -6 to 6
- norm_gain: float32 [2048], replicated, may hold values from 0.1 to 1.9
- w_query_nope: bfloat16 [2048, 2048], P(None, 'tp'), may hold values from -0.125 to 0.125
- w_query_rope: bfloat16 [2048, 1024], P(None, 'tp'), may hold values from -0.125 to 0.125
- w_latent: bfloat16 [2048, 512], replicated, may hold values from -0.125 to 0.125
- w_key_rope: bfloat16 [2048, 64], replicated, may hold values from -0.125 to 0.125
- latent_gain: float32 [512], replicated, may hold values from 0.1 to 1.9
- w_key_up: bfloat16 [16, 128, 512], P('tp'), may hold values from -0.5 to 0.5
- w_value_up: bfloat16 [16, 512, 128], P('tp'), may hold values from -3 to 3
- w_out: bfloat16 [2048, 2048], P(None, 'tp'), may hold values from -0.25 to 0.25
- prompt_latent: bfloat16 [2048, 512], P('kv'), may hold values from -210 to 210
- prompt_rope: bfloat16 [2048, 64], P('kv'), may hold values from -6 to 6
- dec_latent: bfloat16 [8, 1024, 512], P('kv'), may hold values from -210 to 210
- dec_rope: bfloat16 [8, 1024, 64], P('kv'), may hold values from -6 to 6
- dec_lengths: int32 [8], P('kv'), may hold values from 1 to 1024, 4096 in all
Outputs:
- piece_out: bfloat16 [512, 2048], P('kv', 'tp')
- dec_out: bfloat16 [8, 2048], P('kv', 'tp')
Inputs may be any that keep to these rules, and one draw needn't show every extreme that they name: `dec_lengths`: every decoding sequence has at least one live cache slot, and some sequence has all 1024.
All inputs are finite; a program needn't handle non-finite values. No bound on the sum of `dec_lengths` on one device may be relied on, other than what follows from the above.
Results may differ from a plain program's by a relative error of at most 0.025.
Values may be sent and summed in bfloat16 or wider, within the bound.
No kernel may reach another device: no remote copies, remote signals or barrier semaphores. Data moves between devices by JAX's collectives and lax.ppermute only.
A program may use at most 128 MiB of HBM per device.

v0:
```python
import jax
import jax.numpy as jnp
from jax import lax
from jax.sharding import PartitionSpec as P

epsilon = 1e-06
rope_base = 10000.0
masked = -1e30


def normalize(values, gain_vec):
    mean_sq = jnp.mean(values * values, axis=-1, keepdims=True)
    return values * lax.rsqrt(mean_sq + epsilon) * gain_vec


def rotate(values, positions):
    half_dim = values.shape[-1] // 2
    frequency = rope_base ** (-jnp.arange(half_dim, dtype=jnp.float32) / half_dim)
    angles = (positions.astype(jnp.float32)[:, None] * frequency[None, :])[:, None, :]
    cosines = jnp.cos(angles)
    sine_values = jnp.sin(angles)
    front_half = values[..., :half_dim]
    back_half = values[..., half_dim:]
    return jnp.concatenate(
        [
            front_half * cosines - back_half * sine_values,
            front_half * sine_values + back_half * cosines,
        ],
        axis=-1,
    )


def rounded(values):
    return lax.optimization_barrier(values.astype(jnp.bfloat16)).astype(jnp.float32)


def project(
    tokens, positions, norm_gain, w_query_nope, w_query_rope, w_latent, w_key_rope, latent_gain
):
    row_count = tokens.shape[0]
    rope_dim = w_key_rope.shape[1]
    head_count = w_query_rope.shape[1] // rope_dim
    normed = normalize(tokens.astype(jnp.float32), norm_gain).astype(jnp.bfloat16)
    query_nope = jnp.dot(normed, w_query_nope, preferred_element_type=jnp.float32).astype(
        jnp.bfloat16
    )
    query_raw = jnp.dot(normed, w_query_rope, preferred_element_type=jnp.float32).reshape(
        row_count, head_count, rope_dim
    )
    query_rot = rotate(query_raw, positions).astype(jnp.bfloat16)
    latent = normalize(
        jnp.dot(normed, w_latent, preferred_element_type=jnp.float32), latent_gain
    ).astype(jnp.bfloat16)
    key_raw = jnp.dot(normed, w_key_rope, preferred_element_type=jnp.float32)[:, None, :]
    key_rot = rotate(key_raw, positions)[:, 0].astype(jnp.bfloat16)
    return (query_nope, query_rot, latent, key_rot)


def absorb(query_nope, w_key_up):
    head_count, nope_dim, _ = w_key_up.shape
    by_head = query_nope.reshape(query_nope.shape[0], head_count, nope_dim)
    return jnp.einsum("nhd,hdc->nhc", by_head, w_key_up, preferred_element_type=jnp.float32).astype(
        jnp.bfloat16
    )


def shards(
    piece_tokens,
    dec_tokens,
    norm_gain,
    w_query_nope,
    w_query_rope,
    w_latent,
    w_key_rope,
    latent_gain,
    w_key_up,
    w_value_up,
    w_out,
    prompt_latent,
    prompt_rope,
    dec_latent,
    dec_rope,
    dec_lengths,
):
    piece_rows = piece_tokens.shape[0]
    dec_rows = dec_tokens.shape[0]
    cached = prompt_latent.shape[0]
    head_count, latent_dim, value_dim = w_value_up.shape
    rope_dim = w_key_rope.shape[1]
    nope_width = w_query_nope.shape[1]
    score_scale = (w_key_up.shape[1] + rope_dim) ** (-0.5)
    block_index = lax.axis_index("kv")
    prompt_len = cached * lax.axis_size("kv")
    piece_offset = block_index * piece_rows
    positions = jnp.concatenate(
        [prompt_len + piece_offset + jnp.arange(piece_rows, dtype=jnp.int32), dec_lengths]
    )
    tokens = jnp.concatenate([piece_tokens, dec_tokens], axis=0)
    query_nope, query_rot, new_latent, new_rot = project(
        tokens, positions, norm_gain, w_query_nope, w_query_rope, w_latent, w_key_rope, latent_gain
    )
    key_latent = jnp.concatenate([prompt_latent, new_latent[:piece_rows]], axis=0)
    key_rot = jnp.concatenate([prompt_rope, new_rot[:piece_rows]], axis=0)
    column = jnp.arange(key_latent.shape[0], dtype=jnp.int32)
    key_place = piece_offset + column - cached
    rot_width = head_count * rope_dim
    piece_rot = query_rot[:piece_rows].reshape(piece_rows, rot_width)
    outgoing = jnp.concatenate([query_nope[:piece_rows], piece_rot], axis=1)
    shard_rows = lax.all_gather(outgoing, "kv", axis=0, tiled=True)
    row_count = shard_rows.shape[0]
    query_lat = absorb(shard_rows[:, :nope_width], w_key_up)
    query_rope = shard_rows[:, nope_width:].reshape(row_count, head_count, rope_dim)
    score_row_count = query_lat.shape[0]
    scores = (
        jnp.einsum("qhc,kc->qhk", query_lat, key_latent, preferred_element_type=jnp.float32)
        + jnp.einsum("qhr,kr->qhk", query_rope, key_rot, preferred_element_type=jnp.float32)
    ) * score_scale
    query_place = jnp.arange(score_row_count, dtype=jnp.int32)
    visible = (column[None, :] < cached) | (key_place[None, :] <= query_place[:, None])
    scores = jnp.where(visible[:, None, :], scores, masked)
    row_peak = lax.pmax(jnp.max(scores, axis=2).astype(jnp.bfloat16), "kv").astype(jnp.float32)
    weights = jnp.exp(scores - row_peak[:, :, None])
    weight_sum = jnp.sum(weights, axis=2)
    mixed_lat = jnp.einsum(
        "qhk,kc->qhc", weights.astype(jnp.bfloat16), key_latent, preferred_element_type=jnp.float32
    ).astype(jnp.bfloat16)
    partial_value = jnp.einsum(
        "qhc,hcv->qhv", mixed_lat, w_value_up, preferred_element_type=jnp.float32
    )
    all_rows = partial_value.shape[0]
    partial_value = rounded(partial_value).reshape(all_rows, head_count * value_dim)
    summed, denominator = (
        lax.psum_scatter(
            partial_value.astype(jnp.bfloat16), "kv", scatter_dimension=0, tiled=True
        ).astype(jnp.float32),
        lax.psum_scatter(
            weight_sum.astype(jnp.bfloat16), "kv", scatter_dimension=0, tiled=True
        ).astype(jnp.float32),
    )
    piece_attn = (
        summed.reshape(piece_rows, head_count, value_dim) / denominator[:, :, None]
    ).astype(jnp.bfloat16)
    dec_query = absorb(query_nope[piece_rows:], w_key_up)
    dec_rot = query_rot[piece_rows:]
    own_lat = new_latent[piece_rows:]
    own_rot = new_rot[piece_rows:]
    cache_scores = (
        jnp.einsum("bhc,bkc->bhk", dec_query, dec_latent, preferred_element_type=jnp.float32)
        + jnp.einsum("bhr,bkr->bhk", dec_rot, dec_rope, preferred_element_type=jnp.float32)
    ) * score_scale
    live_keys = (
        jnp.arange(dec_latent.shape[1], dtype=jnp.int32)[None, None, :] < dec_lengths[:, None, None]
    )
    cache_scores = jnp.where(live_keys, cache_scores, masked)
    own_scores = (
        jnp.einsum("bhc,bc->bh", dec_query, own_lat, preferred_element_type=jnp.float32)
        + jnp.einsum("bhr,br->bh", dec_rot, own_rot, preferred_element_type=jnp.float32)
    ) * score_scale
    dec_peak = jnp.maximum(jnp.max(cache_scores, axis=2), own_scores)
    cache_w = jnp.exp(cache_scores - dec_peak[:, :, None])
    own_w = jnp.exp(own_scores - dec_peak)
    dec_sum = jnp.sum(cache_w, axis=2) + own_w
    dec_mix = (
        jnp.einsum(
            "bhk,bkc->bhc",
            cache_w.astype(jnp.bfloat16),
            dec_latent,
            preferred_element_type=jnp.float32,
        )
        + rounded(own_w)[:, :, None] * own_lat.astype(jnp.float32)[:, None, :]
    ).astype(jnp.bfloat16)
    dec_value = rounded(
        jnp.einsum("bhc,hcv->bhv", dec_mix, w_value_up, preferred_element_type=jnp.float32)
    )
    dec_attn = (dec_value / dec_sum[:, :, None]).astype(jnp.bfloat16)
    attended = jnp.concatenate(
        [
            piece_attn.reshape(piece_rows, head_count * value_dim),
            dec_attn.reshape(dec_rows, head_count * value_dim),
        ],
        axis=0,
    )
    result = jnp.dot(
        lax.all_gather(attended, "tp", axis=1, tiled=True),
        w_out,
        preferred_element_type=jnp.float32,
    ).astype(jnp.bfloat16)
    return (result[:piece_rows], result[piece_rows:])


def solution(mesh):
    in_specs = (
        P("kv", None),
        P("kv", None),
        P(),
        P(None, "tp"),
        P(None, "tp"),
        P(),
        P(),
        P(),
        P("tp", None, None),
        P("tp", None, None),
        P(None, "tp"),
        P("kv", None),
        P("kv", None),
        P("kv", None, None),
        P("kv", None, None),
        P("kv"),
    )
    out_specs = (P("kv", "tp"), P("kv", "tp"))
    return jax.shard_map(shards, mesh=mesh, in_specs=in_specs, out_specs=out_specs, check_vma=False)
```

profile of v0, /device:TPU:0, one launch (start us, length us, event | category | flops | bytes accessed | tf_op | source)
XLA Modules:
  0.0 113.8 jit_solution(15459763306817569072)
XLA Ops:
  7.3 1.4 %fusion.16 = f32[130]{0:T(256)S(1)} fusion(bf16[2,2048]{1,0:T(2,128)(2,1)} %param.17, bf16[128,2048]{1,0:T(8,128)(2,1)} %param.16), kind=kLoop, calls=%fused_computation.19 | loop fusion | flops 1597310 | bytes 533000 | tf_op jit(solution)/shard_map/reduce_sum | solution.py:12
  8.7 1.9 %convolution_convert_fusion.3 = bf16[130,256]{1,0:T(8,128)(2,1)S(1)} fusion(bf16[2048,256]{1,0:T(8,128)(2,1)} %param.19, f32[2048]{0:T(1024)} %param.18, f32[130]{0:T(256)S(1)} %add_rsqrt_fusion.1, bf16[2,2048]{1,0:T(2,128)(2,1)} %param.17, bf16[128,2048]{1,0:T(8,128)(2,1)} %param.16), kind=kOutput, calls=%fused_computation.17 | convolution fusion | flops 138211840 | bytes 1656328 | tf_op jit(solution)/shard_map/dot_general | solution.py:44
  11.2 0.6 multiply_reduce_fusion
  14.0 16.3 %all_gather.6 = bf16[512,384]{1,0:T(8,128)(2,1)S(1)} all-gather(bf16[128,384]{1,0:T(8,128)(2,1)S(1)} %pad_maximum_fusion.2), channel_id=1, replica_groups=mesh['kv'=4,'tp'=8] {'kv'}, dimensions={0}, use_global_device_ids=true | all-gather | bytes 491520 | tf_op jit(solution)/shard_map/all_gather | solution.py:109
  30.3 0.8 copy.47
  31.3 3.8 %fusion.3 = f32[512,2,640]{2,0,1:T(8,128)} fusion(bf16[2,128,512]{2,1,0:T(8,128)(2,1)S(1)} %copy-done.2, bf16[128,512]{1,0:T(8,128)(2,1)S(1)} %slice.76, bf16[512,512]{1,0:T(8,128)(2,1)} %param.27, bf16[512,384]{1,0:T(8,128)(2,1)S(1)} %all_gather.6), kind=kOutput, calls=%fused_computation.9 | convolution fusion | flops 807141376 | bytes 3801088 | tf_op jit(solution)/shard_map/qhc,kc->qhk/dot_general | solution.py:115
  35.1 4.2 %fusion.68 = (bf16[512,2]{0,1:T(2,128)(2,1)S(1)}, f32[512,2,640]{2,0,1:T(8,128)}) fusion(f32[512,2,640]{2,0,1:T(8,128)} %fusion.3, bf16[512,2,64]{0,2,1:T(8,128)(2,1)} %bitcast.72, bf16[128,64]{0,1:T(8,128)(2,1)S(1)} %fusion.40, bf16[512,64]{0,1:T(8,128)(2,1)} %param.28, pred[512,640]{1,0:T(8,128)(4,1)S(1)} %fusion.9), kind=kOutput, calls=%fused_computation.102 | convolution fusion | flops 86670336 | bytes 5785600 | tf_op jit(solution)/shard_map/qhr,kr->qhk/dot_general | solution.py:116
  39.3 12.4 %pmax.7 = bf16[512,2]{0,1:T(2,128)(2,1)S(1)} all-reduce(bf16[512,2]{0,1:T(2,128)(2,1)S(1)} %get-tuple-element.16), channel_id=1, replica_groups=mesh['kv'=4,'tp'=8] {'kv'}, use_global_device_ids=true, to_apply=%region_3.4 | all-reduce | flops 1024 | bytes 4096 | tf_op jit(solution)/shard_map/pmax | solution.py:121
  51.8 2.4 %fusion = bf16[512,2]{0,1:T(2,128)(2,1)S(1)} fusion(f32[512,2,640]{2,0,1:T(8,128)} %get-tuple-element.17, f32[512,2]{0,1:T(2,128)S(1)} %convert_element_type.109), kind=kLoop, calls=%fused_computation.2 | loop fusion | flops 1309696 | bytes 2627584 | tf_op jit(solution)/shard_map/reduce_sum | solution.py:123
  54.1 0.8 copy.61
  55.0 3.8 %fusion.13 = bf16[512,2,128]{2,0,1:T(8,128)(2,1)} fusion(bf16[2,512,128]{2,1,0:T(8,128)(2,1)} %param.25, f32[512,2,640]{2,0,1:T(8,128)} %get-tuple-element.17, f32[512,2]{0,1:T(2,128)S(1)} %convert_element_type.109, bf16[128,512]{1,0:T(8,128)(2,1)S(1)} %slice.76, bf16[512,512]{1,0:T(8,128)(2,1)S(1)} %copy-done.4), kind=kOutput, calls=%fused_computation.15 | convolution fusion | flops 808583168 | bytes 3805184 | tf_op jit(solution)/shard_map/qhc,hcv->qhv/dot_general | solution.py:127
  58.9 1.1 copy.48
  59.9 0.8 copy.59
  60.8 0.9 fusion.22
  62.0 2.2 %fusion.49 = f32[2,2,1024]{2,1,0:T(2,128)S(1)} fusion(bf16[2,1024,512]{2,1,0:T(8,128)(2,1)} %param.29, bf16[2,2,512]{2,0,1:T(2,128)(2,1)S(1)} %fusion.22), kind=kOutput, calls=%fused_computation.77 | convolution fusion | flops 4194304 | bytes 2117632 | tf_op jit(solution)/shard_map/bhc,bkc->bhk/dot_general | solution.py:148
  65.0 2.0 %fusion.21 = bf16[2,2,512]{2,1,0:T(2,128)(2,1)S(1)} fusion(bf16[2,1024,512]{2,1,0:T(8,128)(2,1)} %param.29, f32[2,2,1024]{2,1,0:T(2,128)S(1)} %get-tuple-element.13, f32[2,2]{1,0:T(2,128)S(1)} %fusion.55, f32[2,512]{1,0:T(2,128)S(1)} %get-tuple-element.6, f32[2,2]{1,0:T(2,128)S(1)} %convert_element_type.123), kind=kOutput, calls=%fused_computation.26 | convolution fusion | flops 4208640 | bytes 2121760 | tf_op jit(solution)/shard_map/bhk,bkc->bhc/dot_general | solution.py:164
  67.5 5.3 %reduce-scatter.9.cloned.1.call-done = bf16[128,2]{1,0:T(8,128)(2,1)} async-done(((bf16[512,2]{1,0:T(8,128)(2,1)}), bf16[128,2]{1,0:T(8,128)(2,1)}) %reduce-scatter.9.cloned.1.call-update) | async-done | bytes 528
  72.8 0.8 copy.62
  73.6 19.7 %reduce-scatter.7.cloned.1.call-done = bf16[128,256]{1,0:T(8,128)(2,1)} async-done(((bf16[512,256]{1,0:T(8,128)(2,1)}), bf16[128,256]{1,0:T(8,128)(2,1)}) %reduce-scatter.7.cloned.1.call-update) | async-done | bytes 65552
  93.3 0.9 copy.60
  94.3 10.9 %all_gather.7 = bf16[130,2048]{0,1:T(8,128)(2,1)S(1)} all-gather(bf16[130,256]{0,1:T(8,128)(2,1)S(1)} %pad_maximum_fusion.1), channel_id=1, replica_groups=mesh['kv'=4,'tp'=8] {'tp'}, dimensions={1}, use_global_device_ids=true | all-gather | bytes 599040 | tf_op jit(solution)/shard_map/all_gather | solution.py:184
  105.2 0.5 convolution_convert_fusion.2
  105.7 0.6 slice.84
  106.4 0.6 slice.85
  (75 shorter events, 4.6 us)
Async XLA Ops:
  7.2 4.0 %copy-start = (bf16[2048,512]{1,0:T(8,128)(2,1)S(1)}, bf16[2048,512]{1,0:T(8,128)(2,1)}, u32[]{:S(2)}) copy-start(bf16[2048,512]{1,0:T(8,128)(2,1)} %param.21) | copy-start | bytes 6291460
  7.2 65.6 %reduce-scatter.9.cloned.1.call-start = ((), (), s32[]{:S(2)}) async-start(), calls=%async_computation.3 | async-start | bytes 163840
  8.6 1.9 %copy-start.3 = (bf16[128,2048]{1,0:T(8,128)(2,1)S(1)}, bf16[128,2048]{1,0:T(8,128)(2,1)}, u32[]{:S(2)}) copy-start(bf16[128,2048]{1,0:T(8,128)(2,1)} %param.16) | copy-start | bytes 1572868
  8.7 1.9 %copy-start.7 = (bf16[2,2048]{1,0:T(2,128)(2,1)S(1)}, bf16[2,2048]{1,0:T(2,128)(2,1)}, u32[]{:S(2)}) copy-start(bf16[2,2048]{1,0:T(2,128)(2,1)} %param.17) | copy-start | bytes 24580
  8.7 1.9 %copy-start.10 = (bf16[2048,128]{1,0:T(8,128)(2,1)S(1)}, bf16[2048,128]{1,0:T(8,128)(2,1)}, u32[]{:S(2)}) copy-start(bf16[2048,128]{1,0:T(8,128)(2,1)} %param.20) | copy-start | bytes 1572868
  8.7 1.9 %copy-start.13 = (f32[2048]{0:T(1024)S(1)}, f32[2048]{0:T(1024)}, u32[]{:S(2)}) copy-start(f32[2048]{0:T(1024)} %param.18) | copy-start | bytes 24580
  10.6 3.4 %copy-start.6 = (bf16[130,256]{1,0:T(8,128)(2,1)}, bf16[130,256]{1,0:T(8,128)(2,1)S(1)}, u32[]{:S(2)}) copy-start(bf16[130,256]{1,0:T(8,128)(2,1)S(1)} %convolution_convert_fusion.3) | copy-start | bytes 199684
  11.2 1.0 copy-start.11
  11.8 0.8 copy-start.9
  11.8 1.3 %copy-start.8 = (f32[512]{0:T(512)S(1)}, f32[512]{0:T(512)}, u32[]{:S(2)}) copy-start(f32[512]{0:T(512)} %param.23) | copy-start | bytes 6148
  13.2 18.1 %copy-start.2 = (bf16[2,128,512]{2,1,0:T(8,128)(2,1)S(1)}, bf16[2,128,512]{2,1,0:T(8,128)(2,1)}, u32[]{:S(2)}) copy-start(bf16[2,128,512]{2,1,0:T(8,128)(2,1)} %param.24) | copy-start | bytes 786436
  51.7 3.3 %copy-start.4 = (bf16[512,512]{1,0:T(8,128)(2,1)S(1)}, bf16[512,512]{1,0:T(8,128)(2,1)}, u32[]{:S(2)}) copy-start(bf16[512,512]{1,0:T(8,128)(2,1)} %param.27) | copy-start | bytes 1572868
  55.0 38.3 %reduce-scatter.7.cloned.1.call-start = ((), (), s32[]{:S(2)}) async-start(), calls=%async_computation.2 | async-start | bytes 327680
  60.8 3.7 %copy-start.12 = (bf16[2,1024,64]{1,2,0:T(8,128)(2,1)S(1)}, bf16[2,1024,64]{1,2,0:T(8,128)(2,1)}, u32[]{:S(2)}) copy-start(bf16[2,1024,64]{1,2,0:T(8,128)(2,1)} %param.30) | copy-start | bytes 786436
  64.2 2.8 %copy-start.5 = (bf16[2,512,128]{2,1,0:T(8,128)(2,1)S(1)}, bf16[2,512,128]{2,1,0:T(8,128)(2,1)}, u32[]{:S(2)}) copy-start(bf16[2,512,128]{2,1,0:T(8,128)(2,1)} %param.25) | copy-start | bytes 786436
  67.0 38.2 %copy-start.1 = (bf16[2048,256]{1,0:T(8,128)(2,1)S(1)}, bf16[2048,256]{1,0:T(8,128)(2,1)}, u32[]{:S(2)}) copy-start(bf16[2048,256]{1,0:T(8,128)(2,1)} %param.26) | copy-start | bytes 3145732
Sparse Core Ops, SparseCore 0:
  55.1 17.6 reduce-scatter.8
  75.1 18.2 reduce-scatter.6
where the time goes:
time: 114 us
  blocking collectives  39.6 us (35%)
  waiting for transfers between devices  25 us (22%)
  matrix products  21.3 us (19%)
  between operations  14.4 us (13%)
  local copies, waits for them, and re-layouts  7.52 us (7%)
  other arithmetic  5.78 us (5%)
    unnamed x4, waiting for transfers between devices  25 us
    all_gather x1, blocking collectives, shards(): shard_rows = lax.all_gather(outgoing, 'kv', axis=0, tiled=True)  16.3 us
    pmax x1, blocking collectives, shards(): lax.pmax(jnp.max(scores, axis=2).astype(jnp.bfloat16), 'kv')  12.4 us
    all_gather x1, blocking collectives, shards(): lax.all_gather(attended, 'tp', axis=1, tiled=True)  10.9 us
    dot_general x1, matrix products, shards(): jnp.einsum('qhr,kr->qhk', query_rope, key_rot, preferred_element_type=jnp...  4.18 us
    dot_general x1, matrix products, shards(): jnp.einsum('qhc,hcv->qhv', mixed_lat, w_value_up, preferred_element_type=...  3.83 us
    dot_general x1, matrix products, shards(): jnp.einsum('qhc,kc->qhk', query_lat, key_latent, preferred_element_type=j...  3.79 us
    unnamed x32, local copies, waits for them, and re-layouts  3.78 us
  transfers between devices with their start and end apart: 2, of which 2 were waited for; matrix products, arithmetic and copies ran while one was open for 12% of the time, Pallas kernels for 0%

commit v1 on v0

--- a/solution.py
+++ b/solution.py
@@ -2,10 +2,24 @@
 import jax.numpy as jnp
 from jax import lax
 from jax.sharding import PartitionSpec as P
+from jax.lax import axis_index, axis_size, ppermute
 
 epsilon = 1e-06
 rope_base = 10000.0
 masked = -1e30
+
+
+def _rest_paths(inp, mesh_ax, d_out):
+    n_slots = axis_size(mesh_ax)
+    val = [(dev_j - 1, dev_j) for dev_j in range(1, n_slots)] + [(n_slots - 1, 0)]
+    even = inp
+    series = [even]
+    for _ in range(n_slots - 1):
+        even = ppermute(even, mesh_ax, val)
+        series += [even]
+    arr_out = jnp.concatenate([*reversed(series)], d_out)
+    extra = jnp.roll(arr_out, (axis_index(mesh_ax) + 1) * even.shape[d_out], d_out)
+    return extra
 
 
 def normalize(values, gain_vec):
@@ -106,7 +120,7 @@
     rot_width = head_count * rope_dim
     piece_rot = query_rot[:piece_rows].reshape(piece_rows, rot_width)
     outgoing = jnp.concatenate([query_nope[:piece_rows], piece_rot], axis=1)
-    shard_rows = lax.all_gather(outgoing, "kv", axis=0, tiled=True)
+    shard_rows = _rest_paths(outgoing, "kv", 0)
     row_count = shard_rows.shape[0]
     query_lat = absorb(shard_rows[:, :nope_width], w_key_up)
     query_rope = shard_rows[:, nope_width:].reshape(row_count, head_count, rope_dim)

time: 114 us -> 123 us (1.079)
  blocking collectives: 39.6 us -> 19.2 us
  waiting for transfers between devices: 25 us -> 42 us
  other arithmetic: 5.78 us -> 11 us
  starting transfers between devices: 0.08 us -> 4.71 us
  local copies, waits for them, and re-layouts: 7.52 us -> 11.4 us
  matrix products: 21.3 us -> 19.1 us
    all_gather x1 -> x0, blocking collectives: 16.3 us -> none  [shards(): shard_rows = lax.all_gather(outgoing, 'kv', axis=0, tiled=True)]
    ppermute x0 -> x3, waiting for transfers between devices: none -> 9.83 us  [_rest_paths(): even = ppermute(even, mesh_ax, val)]
    unnamed x4, waiting for transfers between devices: 25 us -> 32.2 us
    unnamed x32 -> x68, local copies, waits for them, and re-layouts: 3.78 us -> 8.59 us
    ppermute x0 -> x3, starting transfers between devices: none -> 4.63 us  [_rest_paths(): even = ppermute(even, mesh_ax, val)]
    pmax x1, blocking collectives: 12.4 us -> 8.35 us  [shards(): lax.pmax(jnp.max(scores, axis=2).astype(jnp.bfloat16), 'kv')]
    dot_general x1, matrix products: 2.23 us -> 0.64 us  [shards(): jnp.einsum('bhc,bkc->bhk', dec_query, dec_latent, preferred_element_type=...]
  transfers between devices with their start and end apart: 2 -> 5, of which waited for: 2 -> 4; matrix products, arithmetic and copies ran while one was open for 12% -> 12% of each run, Pallas kernels for 0% -> 0%
where the time goes in v1:
time: 123 us; the launch traced here: 122 us
  waiting for transfers between devices  42 us (34%)
  blocking collectives  19.2 us (16%)
  matrix products  19.1 us (16%)
  between operations  14.5 us (12%)
  local copies, waits for them, and re-layouts  11.4 us (9%)
  other arithmetic  11 us (9%)
  starting transfers between devices  4.71 us (4%)
    unnamed x4, waiting for transfers between devices  32.2 us
    all_gather x1, blocking collectives, shards(): lax.all_gather(attended, 'tp', axis=1, tiled=True)  10.9 us
    ppermute x3, waiting for transfers between devices, _rest_paths(): even = ppermute(even, mesh_ax, val)  9.83 us
    unnamed x68, local copies, waits for them, and re-layouts  8.59 us
    pmax x1, blocking collectives, shards(): lax.pmax(jnp.max(scores, axis=2).astype(jnp.bfloat16), 'kv')  8.35 us
    ppermute x3, starting transfers between devices, _rest_paths(): even = ppermute(even, mesh_ax, val)  4.63 us
    dot_general x1, matrix products, shards(): jnp.einsum('qhr,kr->qhk', query_rope, key_rot, preferred_element_type=jnp...  4.05 us
    dot_general x1, matrix products, shards(): jnp.einsum('qhc,kc->qhk', query_lat, key_latent, preferred_element_type=j...  3.72 us
  transfers between devices with their start and end apart: 5, of which 4 were waited for; matrix products, arithmetic and copies ran while one was open for 12% of the time, Pallas kernels for 0%

profile of v1, /device:TPU:0, one launch (start us, length us, event | category | flops | bytes accessed | tf_op | source)
XLA Modules:
  0.0 121.9 jit_solution(7328725645374800780)
XLA Ops:
  7.2 1.4 %fusion.16 = f32[130]{0:T(256)S(1)} fusion(bf16[2,2048]{1,0:T(2,128)(2,1)} %param.17, bf16[128,2048]{1,0:T(8,128)(2,1)} %param.16), kind=kLoop, calls=%fused_computation.19 | loop fusion | flops 1597310 | bytes 533000 | tf_op jit(solution)/shard_map/reduce_sum | solution.py:26
  8.7 1.9 %convolution_convert_fusion.3 = bf16[130,256]{1,0:T(8,128)(2,1)S(1)} fusion(bf16[2048,256]{1,0:T(8,128)(2,1)} %param.19, f32[2048]{0:T(1024)} %param.18, f32[130]{0:T(256)S(1)} %add_rsqrt_fusion.1, bf16[2,2048]{1,0:T(2,128)(2,1)} %param.17, bf16[128,2048]{1,0:T(8,128)(2,1)} %param.16), kind=kOutput, calls=%fused_computation.17 | convolution fusion | flops 138211840 | bytes 1656328 | tf_op jit(solution)/shard_map/dot_general | solution.py:58
  13.0 3.0 %collective-permute-start = (bf16[128,384]{1,0:T(8,128)(2,1)}, bf16[128,384]{1,0:T(8,128)(2,1)}, u32[]{:S(2)}, u32[]{:S(2)}) collective-permute-start(bf16[128,384]{1,0:T(8,128)(2,1)} %pad_maximum_fusion.2), channel_id=1, source_target_pairs={{0,8},{8,16},{16,24},{24,0},{1,9},{9,17},{17,25},{25,1},{2,10},{10... | collective-permute-start | bytes 294920 | tf_op jit(solution)/shard_map/ppermute | solution.py:18
  20.7 1.2 fusion.67
  22.1 1.6 %collective-permute-start.1 = (bf16[128,384]{1,0:T(8,128)(2,1)}, bf16[128,384]{1,0:T(8,128)(2,1)}, u32[]{:S(2)}, u32[]{:S(2)}) collective-permute-start(bf16[128,384]{1,0:T(8,128)(2,1)} %collective-permute-done), channel_id=1, source_target_pairs={{0,8},{8,16},{16,24},{24,0},{1,9},{9,17},{17,25},{25,1},{2,10},{10... | collective-permute-start | bytes 294920 | tf_op jit(solution)/shard_map/ppermute | solution.py:18
  24.9 3.9 %collective-permute-done.1 = bf16[128,384]{1,0:T(8,128)(2,1)} collective-permute-done((bf16[128,384]{1,0:T(8,128)(2,1)}, bf16[128,384]{1,0:T(8,128)(2,1)}, u32[]{:S(2)}, u32[]{:S(2)}) %collective-permute-start.1) | collective-permute-done | bytes 98336 | tf_op jit(solution)/shard_map/ppermute | solution.py:18
  29.5 5.9 %collective-permute-done.2 = bf16[128,384]{1,0:T(8,128)(2,1)S(1)} collective-permute-done((bf16[128,384]{1,0:T(8,128)(2,1)}, bf16[128,384]{1,0:T(8,128)(2,1)S(1)}, u32[]{:S(2)}, u32[]{:S(2)}) %collective-permute-start.2) | collective-permute-done | bytes 98336 | tf_op jit(solution)/shard_map/ppermute | solution.py:18
  35.5 0.9 constant_dynamic-update-slice_fusion.6
  36.4 0.9 constant_dynamic-update-slice_fusion.5
  38.1 0.9 constant_dynamic-update-slice_fusion.2
  39.0 0.9 constant_dynamic-update-slice_fusion.1
  40.7 0.9 copy-done.8
  42.4 3.7 %fusion.3 = f32[512,2,640]{2,0,1:T(8,128)} fusion(bf16[2,128,512]{2,1,0:T(8,128)(2,1)S(1)} %copy-done.2, bf16[128,512]{1,0:T(8,128)(2,1)S(1)} %slice.75, bf16[512,512]{1,0:T(8,128)(2,1)S(1)} %copy-done.5, bf16[1024,384]{1,0:T(8,128)(2,1)} %copy-done.8, s32[]{:T(128)S(6)} %select_n.22), kind=kOutput, calls=%fused_computation.9 | convolution fusion | flops 807141376 | bytes 3801092 | tf_op jit(solution)/shard_map/qhc,kc->qhk/dot_general | solution.py:129
  46.1 4.0 %fusion.68 = (bf16[512,2]{0,1:T(2,128)(2,1)S(1)}, f32[512,2,640]{2,0,1:T(8,128)}) fusion(f32[512,2,640]{2,0,1:T(8,128)} %fusion.3, bf16[512,2,64]{0,2,1:T(8,128)(2,1)S(1)} %bitcast.72, bf16[128,64]{0,1:T(8,128)(2,1)S(1)} %fusion.40, bf16[512,64]{0,1:T(8,128)(2,1)S(1)} %copy-done.14, pred[512,640]{1,0:T(8,128)(4,1)S(1)} %fusion.9), kind=kOutput, calls=%fused_computation.110 | convolution fusion | flops 86670336 | bytes 5785600 | tf_op jit(solution)/shard_map/qhr,kr->qhk/dot_general | solution.py:130
  50.2 8.3 %pmax.7 = bf16[512,2]{0,1:T(2,128)(2,1)S(1)} all-reduce(bf16[512,2]{0,1:T(2,128)(2,1)S(1)} %get-tuple-element.16), channel_id=1, replica_groups=mesh['kv'=4,'tp'=8] {'kv'}, use_global_device_ids=true, to_apply=%region_3.4 | all-reduce | flops 1024 | bytes 4096 | tf_op jit(solution)/shard_map/pmax | solution.py:135
  58.5 2.4 %fusion = bf16[512,2]{0,1:T(2,128)(2,1)S(1)} fusion(f32[512,2,640]{2,0,1:T(8,128)} %get-tuple-element.17, f32[512,2]{0,1:T(2,128)S(1)} %convert_element_type.109), kind=kLoop, calls=%fused_computation.2 | loop fusion | flops 1309696 | bytes 2627584 | tf_op jit(solution)/shard_map/reduce_sum | solution.py:137
  61.8 3.1 %fusion.13 = bf16[512,2,128]{2,0,1:T(8,128)(2,1)S(1)} fusion(bf16[2,512,128]{2,1,0:T(8,128)(2,1)S(1)} %copy-done.9, f32[512,2,640]{2,0,1:T(8,128)} %get-tuple-element.17, f32[512,2]{0,1:T(2,128)S(1)} %convert_element_type.109, bf16[128,512]{1,0:T(8,128)(2,1)S(1)} %slice.75, bf16[512,512]{1,0:T(8,128)(2,1)S(1)} %copy-done.5), kind=kOutput, calls=%fused_computation.15 | convolution fusion | flops 808583168 | bytes 3805184 | tf_op jit(solution)/shard_map/qhc,hcv->qhv/dot_general | solution.py:141
  65.1 0.8 copy.59
  66.0 2.1 %fusion.21 = bf16[2,2,512]{2,1,0:T(2,128)(2,1)S(1)} fusion(bf16[2,1024,512]{2,1,0:T(8,128)(2,1)} %param.29, f32[2,2,1024]{2,1,0:T(2,128)S(1)} %copy-done.16, f32[2,2]{1,0:T(2,128)S(1)} %copy-done.19, f32[2,512]{1,0:T(2,128)S(1)} %copy-done.17, f32[2,2]{1,0:T(2,128)S(1)} %copy-done.24), kind=kOutput, calls=%fused_computation.26 | convolution fusion | flops 4208640 | bytes 2121760 | tf_op jit(solution)/shard_map/bhk,bkc->bhc/dot_general | solution.py:178
  68.5 12.5 %reduce-scatter.9.cloned.1.call-done = bf16[128,2]{1,0:T(8,128)(2,1)} async-done(((bf16[512,2]{1,0:T(8,128)(2,1)}), bf16[128,2]{1,0:T(8,128)(2,1)}) %reduce-scatter.9.cloned.1.call-update) | async-done | bytes 528
  81.0 0.8 copy.62
  81.9 19.6 %reduce-scatter.7.cloned.1.call-done = bf16[128,256]{1,0:T(8,128)(2,1)} async-done(((bf16[512,256]{1,0:T(8,128)(2,1)}), bf16[128,256]{1,0:T(8,128)(2,1)}) %reduce-scatter.7.cloned.1.call-update) | async-done | bytes 65552
  101.5 0.9 copy.60
  102.5 10.9 %all_gather.3 = bf16[130,2048]{0,1:T(8,128)(2,1)S(1)} all-gather(bf16[130,256]{0,1:T(8,128)(2,1)S(1)} %pad_maximum_fusion.1), channel_id=1, replica_groups=mesh['kv'=4,'tp'=8] {'tp'}, dimensions={1}, use_global_device_ids=true | all-gather | bytes 599040 | tf_op jit(solution)/shard_map/all_gather | solution.py:198
  (118 shorter events, 14.7 us)
Async XLA Ops:
  7.2 9.9 %copy-start = (bf16[2048,512]{1,0:T(8,128)(2,1)S(1)}, bf16[2048,512]{1,0:T(8,128)(2,1)}, u32[]{:S(2)}) copy-start(bf16[2048,512]{1,0:T(8,128)(2,1)} %param.21) | copy-start | bytes 6291460
  7.2 73.9 %reduce-scatter.9.cloned.1.call-start = ((), (), s32[]{:S(2)}) async-start(), calls=%async_computation.3 | async-start | bytes 163840
  8.6 1.9 %copy-start.4 = (bf16[128,2048]{1,0:T(8,128)(2,1)S(1)}, bf16[128,2048]{1,0:T(8,128)(2,1)}, u32[]{:S(2)}) copy-start(bf16[128,2048]{1,0:T(8,128)(2,1)} %param.16) | copy-start | bytes 1572868
  8.6 1.9 %copy-start.20 = (bf16[2,2048]{1,0:T(2,128)(2,1)S(1)}, bf16[2,2048]{1,0:T(2,128)(2,1)}, u32[]{:S(2)}) copy-start(bf16[2,2048]{1,0:T(2,128)(2,1)} %param.17) | copy-start | bytes 24580
  8.7 1.9 %copy-start.26 = (bf16[2048,128]{1,0:T(8,128)(2,1)S(1)}, bf16[2048,128]{1,0:T(8,128)(2,1)}, u32[]{:S(2)}) copy-start(bf16[2048,128]{1,0:T(8,128)(2,1)} %param.20) | copy-start | bytes 1572868
  8.7 1.9 %copy-start.28 = (f32[2048]{0:T(1024)S(1)}, f32[2048]{0:T(1024)}, u32[]{:S(2)}) copy-start(f32[2048]{0:T(1024)} %param.18) | copy-start | bytes 24580
  11.0 5.9 %copy-start.2 = (bf16[2,128,512]{2,1,0:T(8,128)(2,1)S(1)}, bf16[2,128,512]{2,1,0:T(8,128)(2,1)}, u32[]{:S(2)}) copy-start(bf16[2,128,512]{2,1,0:T(8,128)(2,1)} %param.24) | copy-start | bytes 786436
  12.3 5.3 %copy-start.6 = (bf16[128,128]{1,0:T(8,128)(2,1)}, bf16[128,128]{1,0:T(8,128)(2,1)S(1)}, u32[]{:S(2)}) copy-start(bf16[128,128]{1,0:T(8,128)(2,1)S(1)} %copy.45) | copy-start | bytes 98308
  13.0 9.1 %collective-permute-start = (bf16[128,384]{1,0:T(8,128)(2,1)}, bf16[128,384]{1,0:T(8,128)(2,1)}, u32[]{:S(2)}, u32[]{:S(2)}) collective-permute-start(bf16[128,384]{1,0:T(8,128)(2,1)} %pad_maximum_fusion.2), channel_id=1, source_target_pairs={{0,8},{8,16},{16,24},{24,0},{1,9},{9,17},{17,25},{25,1},{2,10},{10... | collective-permute-start | bytes 294920 | tf_op jit(solution)/shard_map/ppermute | solution.py:18
  16.2 4.0 %copy-start.13 = (bf16[130,2,64]{2,1,0:T(2,128)(2,1)}, bf16[130,2,64]{2,1,0:T(2,128)(2,1)S(1)}, u32[]{:S(2)}) copy-start(bf16[130,2,64]{2,1,0:T(2,128)(2,1)S(1)} %pad_maximum_fusion.3) | copy-start | bytes 99844
  17.0 1.6 %copy-start.1 = (bf16[2,1024,512]{2,1,0:T(8,128)(2,1)S(1)}, bf16[2,1024,512]{2,1,0:T(8,128)(2,1)}, u32[]{:S(2)}) copy-start(bf16[2,1024,512]{2,1,0:T(8,128)(2,1)} %param.29) | copy-start | bytes 6291460
  17.7 1.8 %copy-start.27 = (bf16[2048,64]{0,1:T(8,128)(2,1)S(1)}, bf16[2048,64]{0,1:T(8,128)(2,1)}, u32[]{:S(2)}) copy-start(bf16[2048,64]{0,1:T(8,128)(2,1)} %param.22) | copy-start | bytes 786436
  21.9 1.8 %copy-start.15 = (f32[2,2,1024]{2,1,0:T(2,128)}, f32[2,2,1024]{2,1,0:T(2,128)S(1)}, u32[]{:S(2)}) copy-start(f32[2,2,1024]{2,1,0:T(2,128)S(1)} %get-tuple-element.13) | copy-start | bytes 49156
  21.9 20.5 %copy-start.5 = (bf16[512,512]{1,0:T(8,128)(2,1)S(1)}, bf16[512,512]{1,0:T(8,128)(2,1)}, u32[]{:S(2)}) copy-start(bf16[512,512]{1,0:T(8,128)(2,1)} %param.27) | copy-start | bytes 1572868
  21.9 1.8 %copy-start.18 = (f32[2,2]{1,0:T(2,128)}, f32[2,2]{1,0:T(2,128)S(1)}, u32[]{:S(2)}) copy-start(f32[2,2]{1,0:T(2,128)S(1)} %fusion.55) | copy-start | bytes 52
  22.1 6.7 %collective-permute-start.1 = (bf16[128,384]{1,0:T(8,128)(2,1)}, bf16[128,384]{1,0:T(8,128)(2,1)}, u32[]{:S(2)}, u32[]{:S(2)}) collective-permute-start(bf16[128,384]{1,0:T(8,128)(2,1)} %collective-permute-done), channel_id=1, source_target_pairs={{0,8},{8,16},{16,24},{24,0},{1,9},{9,17},{17,25},{25,1},{2,10},{10... | collective-permute-start | bytes 294920 | tf_op jit(solution)/shard_map/ppermute | solution.py:18
  28.8 6.6 %collective-permute-start.2 = (bf16[128,384]{1,0:T(8,128)(2,1)}, bf16[128,384]{1,0:T(8,128)(2,1)S(1)}, u32[]{:S(2)}, u32[]{:S(2)}) collective-permute-start(bf16[128,384]{1,0:T(8,128)(2,1)} %collective-permute-done.1), channel_id=1, source_target_pairs={{0,8},{8,16},{16,24},{24,0},{1,9},{9,17},{17,25},{25,1},{2,10},{10... | collective-permute-start | bytes 294920 | tf_op jit(solution)/shard_map/ppermute | solution.py:18
  42.4 3.7 %copy-start.7 = (bf16[512,128]{0,1:T(8,128)(2,1)S(1)}, bf16[512,128]{0,1:T(8,128)(2,1)}, u32[]{:S(2)}) copy-start(bf16[512,128]{0,1:T(8,128)(2,1)} %copy.47) | copy-start | bytes 393220
  42.4 3.7 %copy-start.14 = (bf16[512,64]{0,1:T(8,128)(2,1)S(1)}, bf16[512,64]{0,1:T(8,128)(2,1)}, u32[]{:S(2)}) copy-start(bf16[512,64]{0,1:T(8,128)(2,1)} %param.28) | copy-start | bytes 196612
  58.5 3.3 %copy-start.9 = (bf16[2,512,128]{2,1,0:T(8,128)(2,1)S(1)}, bf16[2,512,128]{2,1,0:T(8,128)(2,1)}, u32[]{:S(2)}) copy-start(bf16[2,512,128]{2,1,0:T(8,128)(2,1)} %param.25) | copy-start | bytes 786436
  61.7 39.8 %reduce-scatter.7.cloned.1.call-start = ((), (), s32[]{:S(2)}) async-start(), calls=%async_computation.2 | async-start | bytes 327680
  65.9 2.1 %copy-start.10 = (bf16[2,512,128]{2,1,0:T(8,128)(2,1)S(1)}, bf16[2,512,128]{2,1,0:T(8,128)(2,1)}, u32[]{:S(2)}) copy-start(bf16[2,512,128]{2,1,0:T(8,128)(2,1)} %param.25) | copy-start | bytes 786436
  65.9 2.3 %copy-start.21 = (f32[2,2]{1,0:T(2,128)S(1)}, f32[2,2]{1,0:T(2,128)}, u32[]{:S(2)}) copy-start(f32[2,2]{1,0:T(2,128)} %get-tuple-element.2) | copy-start | bytes 52
  68.0 45.4 %copy-start.3 = (bf16[2048,256]{1,0:T(8,128)(2,1)S(1)}, bf16[2048,256]{1,0:T(8,128)(2,1)}, u32[]{:S(2)}) copy-start(bf16[2048,256]{1,0:T(8,128)(2,1)} %param.26) | copy-start | bytes 3145732
  (10 other events, 8.7 us)
Sparse Core Ops, SparseCore 0:
  61.8 19.1 reduce-scatter.8
  83.3 18.1 reduce-scatter.6
